TPU v7x, 32 devices: a whole 2x2x4 slice. The times are simulated.
32 devices in a mesh: ep: 4 (over y, x), tp: 8 (over z, core).
Axes of the slice: x: 2, y: 2, z: 4, core: 2. Of those that a mesh axis runs over, the one named last changes fastest.
Arguments:
- features: bfloat16 [64, 1024], P('ep', 'tp'), may hold values from -6 to 6
- key_table: bfloat16 [65536, 1024], P('ep', 'tp'), may hold values from -0.1875 to 0.1875
- value_table: bfloat16 [65536, 1024], P('ep', 'tp'), may hold values from -6 to 6
- chosen: int32 [64, 4, 16], P('ep'), may hold values from 0 to 65535
- scores: float32 [64, 4, 16], P('ep'), may hold values from -8 to 8
Outputs:
- mixed: bfloat16 [64, 1024], P('ep', 'tp')
Inputs may be any that keep to these rules, and one draw needn't show every extreme that they name: Every chosen row is a row of the tables, 0 to 65535; rows may repeat, and a few rows are far more popular than the rest.
All inputs are finite; a program needn't handle non-finite values.
Results may differ from a plain program's by a relative error of at most 0.0065.
Values may be sent and summed in bfloat16 or wider, within the bound.
A program may use at most 64 MiB of HBM per device.

v0:
```python
import jax
import jax.numpy as jnp
from jax import lax
from jax.sharding import PartitionSpec as P


def in_blocks(func, arrays):
    total = arrays[0].shape[0]
    width = 32 if total % 32 == 0 else total
    count = total // width
    if count == 1:
        return func(arrays)
    shaped = tuple((item.reshape((count, width) + item.shape[1:]) for item in arrays))
    result = lax.map(func, shaped)
    return result.reshape((total,) + result.shape[2:])


def shards(features, key_table, value_table, chosen, scores):
    table_rows = key_table.shape[0]
    head_count = chosen.shape[1]
    top_count = chosen.shape[2]
    first_row = lax.axis_index("ep") * table_rows
    gate_weights = jax.nn.softmax(scores, axis=-1)
    chosen_all = lax.all_gather(chosen, "ep", axis=0, tiled=True)
    gates_all = lax.all_gather(gate_weights, "ep", axis=0, tiled=True)
    shifted = chosen_all - first_row
    owned_mask = (shifted >= 0) & (shifted < table_rows)
    local_rows = jnp.clip(shifted, 0, table_rows - 1).reshape(shifted.shape[0], -1)

    def dots_block(pair):
        token_block, picked = pair
        dense = lax.dot_general(
            token_block, key_table, (((1,), (1,)), ((), ())), preferred_element_type=jnp.float32
        )
        return jnp.take_along_axis(dense, picked, axis=1)

    def partial_dots(token_block):
        row_count = token_block.shape[0]
        picked = lax.slice_in_dim(local_rows, 0, row_count, axis=0)
        keep_mask = lax.slice_in_dim(owned_mask, 0, row_count, axis=0)
        products = in_blocks(dots_block, (token_block, picked))
        return jnp.where(keep_mask.reshape(row_count, -1), products, 0.0)

    partial_value = partial_dots(lax.all_gather(features, "ep", axis=0, tiled=True))
    partial_value = partial_value.reshape(-1, head_count, top_count)
    products = lax.psum(partial_value, "tp")
    row_weights = (gates_all * jax.nn.gelu(products, approximate=False)).astype(jnp.bfloat16)
    row_weights = jnp.where(owned_mask, row_weights, jnp.zeros_like(row_weights))
    flat_weights = row_weights.reshape(row_weights.shape[0], -1)

    def value_block(pair):
        block_weights, picked = pair
        width = picked.shape[0]
        token_ids = lax.broadcasted_iota(jnp.int32, picked.shape, 0)
        dense = (
            jnp.zeros((width, table_rows), jnp.float32)
            .at[token_ids, picked]
            .add(block_weights.astype(jnp.float32))
        )
        upper = dense.astype(jnp.bfloat16)
        lower = (dense - upper.astype(jnp.float32)).astype(jnp.bfloat16)
        summed = jnp.dot(upper, value_table, preferred_element_type=jnp.float32)
        return summed + jnp.dot(lower, value_table, preferred_element_type=jnp.float32)

    def owner_term(row_count):
        picked = lax.slice_in_dim(local_rows, 0, row_count, axis=0)
        block_weights = lax.slice_in_dim(flat_weights, 0, row_count, axis=0)
        return in_blocks(value_block, (block_weights, picked))

    summed = lax.psum_scatter(
        owner_term(lax.axis_size("ep") * features.shape[0]), "ep", scatter_dimension=0, tiled=True
    )
    return summed.astype(jnp.bfloat16)


def solution(mesh):
    return jax.shard_map(
        shards,
        mesh=mesh,
        in_specs=(
            P("ep", "tp"),
            P("ep", "tp"),
            P("ep", "tp"),
            P("ep", None, None),
            P("ep", None, None),
        ),
        out_specs=P("ep", "tp"),
        check_vma=False,
    )
```

profile of v0, /device:TPU:0, one launch (start us, length us, event | category | flops | bytes accessed | tf_op | source)
XLA Modules:
  0.0 150.2 jit_solution(2925781054300284029)
XLA Ops:
  0.0 10.2 %all_gather.9 = s32[64,4,16]{2,1,0:T(4,128)S(1)} all-gather(s32[16,4,16]{2,1,0:T(4,128)} %param.12), channel_id=1, replica_groups=mesh['ep'=4,'tp'=8] {'ep'}, dimensions={0}, use_global_device_ids=true | all-gather | bytes 20480 | tf_op jit(solution)/shard_map/all_gather | solution.py:24
  10.5 7.9 %all_gather.11 = bf16[64,128]{1,0:T(8,128)(2,1)S(1)} all-gather(bf16[16,128]{1,0:T(8,128)(2,1)} %param.9), channel_id=1, replica_groups=mesh['ep'=4,'tp'=8] {'ep'}, dimensions={0}, use_global_device_ids=true | all-gather | bytes 20480 | tf_op jit(solution)/shard_map/all_gather | solution.py:44
  18.4 41.1 %while.20 = (s32[]{:T(128)}, f32[2,32,64]{2,1,0:T(8,128)S(1)}, s32[2,32,64]{2,1,0:T(8,128)S(1)}, bf16[2,32,128]{2,1,0:T(8,128)(2,1)S(1)}, bf16[16384,128]{1,0:T(8,128)(2,1)}, /*index=5*/s32[]{:T(128)}) while((s32[]{:T(128)}, f32[2,32,64]{2,1,0:T(8,128)S(1)}, s32[2,32,64]{2,1,0:T(8,128)S(1)}, bf16[2,32,128]{2,1,0:T(8,128)(2,1)S(1)}, ...), condition=%wide.region_3.4_spmd, body=%wide.region_2.3_spmd.sunk | while | flops 134248448 | bytes 6430801 | solution.py:14
  18.4 3.7 %fusion.47 = f32[32,16384]{1,0:T(8,128)S(1)} fusion(bf16[16384,128]{1,0:T(8,128)(2,1)} %get-tuple-element.181, bf16[2,32,128]{2,1,0:T(8,128)(2,1)S(1)} %get-tuple-element.180, s32[]{:T(128)} %get-tuple-element.171), kind=kOutput, calls=%fused_computation.8.clone.1 | convolution fusion | flops 134217728 | bytes 6299652 | tf_op jit(solution)/shard_map/while/body/eval_jaxpr/dot_general | solution.py:32
  22.3 16.6 %gather_fusion = f32[2048]{0:T(1024)S(1)} fusion(f32[32,16384]{1,0:T(8,128)S(1)} %fusion.47, s32[2048]{0:T(1024)S(1)} %reshape.128), kind=kCustom, calls=%fused_computation.clone.1 | custom fusion | bytes 32768 | tf_op jit(solution)/shard_map/while/body/eval_jaxpr/jit(take_along_axis)/gather | solution.py:35
  39.0 3.7 %fusion.47 = f32[32,16384]{1,0:T(8,128)S(1)} fusion(bf16[16384,128]{1,0:T(8,128)(2,1)} %get-tuple-element.181, bf16[2,32,128]{2,1,0:T(8,128)(2,1)S(1)} %get-tuple-element.180, s32[]{:T(128)} %get-tuple-element.171), kind=kOutput, calls=%fused_computation.8.clone.1 | convolution fusion | flops 134217728 | bytes 6299652 | tf_op jit(solution)/shard_map/while/body/eval_jaxpr/dot_general | solution.py:32
  42.8 16.6 %gather_fusion = f32[2048]{0:T(1024)S(1)} fusion(f32[32,16384]{1,0:T(8,128)S(1)} %fusion.47, s32[2048]{0:T(1024)S(1)} %reshape.128), kind=kCustom, calls=%fused_computation.clone.1 | custom fusion | bytes 32768 | tf_op jit(solution)/shard_map/while/body/eval_jaxpr/jit(take_along_axis)/gather | solution.py:35
  59.8 26.0 %psum.7 = f32[64,4,16]{0,2,1:T(8,128)S(1)} all-reduce(f32[64,4,16]{0,2,1:T(8,128)S(1)} %get-tuple-element.101), channel_id=1, replica_groups=mesh['ep'=4,'tp'=8] {'tp'}, use_global_device_ids=true, to_apply=%region_4.5 | all-reduce | flops 4096 | bytes 32768 | tf_op jit(solution)/shard_map/psum | solution.py:46
  85.8 0.2 fusion.17
  86.0 7.7 %all_gather.10 = f32[64,4,16]{2,1,0:T(4,128)S(1)} all-gather(f32[16,4,16]{2,1,0:T(4,128)S(1)} %fusion.17), channel_id=1, replica_groups=mesh['ep'=4,'tp'=8] {'ep'}, dimensions={0}, use_global_device_ids=true | all-gather | bytes 20480 | tf_op jit(solution)/shard_map/all_gather | solution.py:25
  94.0 39.5 %while.21 = (s32[]{:T(128)}, f32[2,32,128]{2,1,0:T(8,128)S(1)}, s32[2,32,64]{2,1,0:T(8,128)S(1)}, bf16[2,32,64]{2,1,0:T(8,128)(2,1)S(1)}, bf16[16384,128]{1,0:T(...) while((s32[]{:T(128)}, f32[2,32,128]{2,1,0:T(8,128)S(1)}, ...), condition=%wide.region_7.8_spmd, body=%wide.region_5.7_spmd.sunk | while | flops 271101952 | bytes 35831960 | solution.py:14
  94.4 13.3 %scatter_custom_fusion.5 = f32[524288]{0:T(1024)} fusion(s32[2048]{0:T(1024)S(1)} %reshape.131, f32[2048]{0:T(1024)S(1)} %reshape.132, f32[]{:T(128)} %constant.53.clone.1..sunk), kind=kCustom, calls=%fused_computation.16.clone.1 | custom fusion | flops 2048 | bytes 2097156 | tf_op jit(solution)/shard_map/while
  107.7 1.7 %reshape.133 = f32[32,16384]{1,0:T(8,128)S(1)} reshape(f32[524288]{0:T(1024)} %scatter_custom_fusion.5) | data formatting | bytes 4194304 | tf_op jit(solution)/shard_map/while/body/eval_jaxpr/scatter-add | solution.py:58
  109.4 3.1 %fusion.53 = f32[32,128]{1,0:T(8,128)S(1)} fusion(bf16[16384,128]{1,0:T(8,128)(2,1)} %get-tuple-element.205, f32[32,16384]{1,0:T(8,128)S(1)} %reshape.133), kind=kOutput, calls=%fused_computation.19.clone.1 | convolution fusion | flops 134742016 | bytes 6307840 | tf_op jit(solution)/shard_map/while/body/eval_jaxpr/dot_general | solution.py:62
  112.5 0.3 copy-done
  112.9 0.8 fusion.54
  114.0 13.5 %scatter_custom_fusion.5 = f32[524288]{0:T(1024)} fusion(s32[2048]{0:T(1024)S(1)} %reshape.131, f32[2048]{0:T(1024)S(1)} %reshape.132, f32[]{:T(128)} %constant.53.clone.1..sunk), kind=kCustom, calls=%fused_computation.16.clone.1 | custom fusion | flops 2048 | bytes 2097156 | tf_op jit(solution)/shard_map/while
  127.5 1.7 %reshape.133 = f32[32,16384]{1,0:T(8,128)S(1)} reshape(f32[524288]{0:T(1024)} %scatter_custom_fusion.5) | data formatting | bytes 4194304 | tf_op jit(solution)/shard_map/while/body/eval_jaxpr/scatter-add | solution.py:58
  129.3 3.1 %fusion.53 = f32[32,128]{1,0:T(8,128)S(1)} fusion(bf16[16384,128]{1,0:T(8,128)(2,1)} %get-tuple-element.205, f32[32,16384]{1,0:T(8,128)S(1)} %reshape.133), kind=kOutput, calls=%fused_computation.19.clone.1 | convolution fusion | flops 134742016 | bytes 6307840 | tf_op jit(solution)/shard_map/while/body/eval_jaxpr/dot_general | solution.py:62
  132.4 0.3 copy-done
  132.7 0.8 fusion.54
  133.5 14.8 %all-reduce = bf16[64,128]{1,0:T(8,128)(2,1)S(1)} all-reduce(f32[64,128]{1,0:T(8,128)S(1)} %bitcast.41), channel_id=2, replica_groups=mesh['ep'=4,'tp'=8] {'ep'}, use_global_device_ids=true, to_apply=%region_8.9.clone | all-reduce | flops 8192 | bytes 49152
  148.4 0.6 dynamic-slice
  149.6 0.6 dynamic-slice_convert_fusion.1
  (47 shorter events, 1.9 us)
Async XLA Ops:
  18.4 67.4 %copy-start.3 = (f32[16,4,16]{2,1,0:T(4,128)S(1)}, f32[16,4,16]{2,1,0:T(4,128)}, u32[]{:S(2)}) copy-start(f32[16,4,16]{2,1,0:T(4,128)} %param.13) | copy-start | bytes 12292
  18.4 75.6 %copy-start.1 = (s32[2]{0:T(128)S(1)}, s32[2]{0:T(128)}, u32[]{:S(2)}) copy-start(s32[2]{0:T(128)} %constant.199) | copy-start | bytes 28
  18.4 75.6 %copy-start.2 = (s32[2]{0:T(128)S(1)}, s32[2]{0:T(128)}, u32[]{:S(2)}) copy-start(s32[2]{0:T(128)} %constant.200) | copy-start | bytes 28
  94.0 54.3 %copy-start.4 = (u32[32]{0:T(128)S(1)}, u32[32]{0:T(128)}, u32[]{:S(2)}) copy-start(u32[32]{0:T(128)} %constant.148) | copy-start | bytes 388
  109.4 3.5 %copy-start = (bf16[16384,128]{1,0:T(8,128)(2,1)S(1)}, bf16[16384,128]{1,0:T(8,128)(2,1)}, u32[]{:S(2)}) copy-start(bf16[16384,128]{1,0:T(8,128)(2,1)} %get-tuple-element.205) | copy-start | bytes 12582916 | tf_op jit(solution)/shard_map/while
  129.3 3.5 %copy-start = (bf16[16384,128]{1,0:T(8,128)(2,1)S(1)}, bf16[16384,128]{1,0:T(8,128)(2,1)}, u32[]{:S(2)}) copy-start(bf16[16384,128]{1,0:T(8,128)(2,1)} %get-tuple-element.205) | copy-start | bytes 12582916 | tf_op jit(solution)/shard_map/while
where the time goes:
time: 151 us; the launch traced here: 150 us
  blocking collectives  66.6 us (44%)
  local copies, waits for them, and re-layouts  40 us (26%)
  other arithmetic  27.5 us (18%)
  matrix products  15.2 us (10%)
    gather x6, local copies, waits for them, and re-layouts, dots_block(): return jnp.take_along_axis(dense, picked, axis=1)  33.6 us
    while x8, other arithmetic  27.1 us
    psum x1, blocking collectives, shards(): products = lax.psum(partial_value, 'tp')  26 us
    unnamed x1, blocking collectives  14.8 us
    all_gather x1, blocking collectives, shards(): chosen_all = lax.all_gather(chosen, 'ep', axis=0, tiled=True)  10.2 us
    all_gather x1, blocking collectives, shards(): lax.all_gather(features, 'ep', axis=0, tiled=True)  7.93 us
    all_gather x1, blocking collectives, shards(): gates_all = lax.all_gather(gate_weights, 'ep', axis=0, tiled=True)  7.69 us
    dot_general x2, matrix products, dots_block(): lax.dot_general(token_block, key_table, (((1,), (1,)), ((), ())), preferr...  7.46 us

commit v1 on v0

v1 whole, which is shorter than its diff:
```python
import functools

import jax
import jax.numpy as jnp
from jax import lax
from jax.experimental import pallas as pl
from jax.experimental.pallas import tpu as pltpu
from jax.sharding import PartitionSpec as P

LANES = 128
GROUP = 16
MESH = pl.DeviceIdType.MESH


def matmul_nt(left, right):
    return lax.dot_general(
        left, right, (((1,), (1,)), ((), ())), preferred_element_type=jnp.float32
    )


def split_terms(value):
    upper = value.astype(jnp.bfloat16)
    lower = (value - upper.astype(jnp.float32)).astype(jnp.bfloat16)
    return upper, lower


def kernel(
    ep_size,
    tp_size,
    features_hbm,
    key_hbm,
    value_hbm,
    chosen_hbm,
    scores_hbm,
    out_ref,
    features,
    chosen,
    scores,
    key,
    value,
    dense,
    picks,
    partial,
    weights,
    summed,
    landed,
    local_sem,
    send_sem,
    recv_sem,
    tp_send,
    tp_recv,
    out_send,
    out_recv,
):
    my_ep = lax.axis_index("ep")
    my_tp = lax.axis_index("tp")
    table_rows = key.shape[0]
    blocks = table_rows // LANES
    own_tokens, heads, top = chosen_hbm.shape
    tokens = ep_size * own_tokens
    half = tokens // 2
    per_token = heads * top
    width = 2 * per_token

    def token_slot(ref, index):
        return ref.at[pl.ds(index * own_tokens, own_tokens)]

    small = (
        (features_hbm, features),
        (chosen_hbm, chosen),
        (scores_hbm, scores),
    )
    small_copies = []
    for number, (source, target) in enumerate(small):
        copy = pltpu.make_async_copy(source, token_slot(target, my_ep), local_sem.at[number])
        copy.start()
        small_copies.append(copy)
    key_copy = pltpu.make_async_copy(key_hbm, key, local_sem.at[3])
    key_copy.start()
    value_copy = pltpu.make_async_copy(value_hbm, value, local_sem.at[4])
    value_copy.start()

    barrier = pltpu.get_barrier_semaphore()
    for step in range(1, ep_size):
        pl.semaphore_signal(
            barrier, inc=1, device_id=(lax.rem(my_ep + step, ep_size), my_tp), device_id_type=MESH
        )
    for step in range(1, tp_size):
        pl.semaphore_signal(
            barrier, inc=1, device_id=(my_ep, lax.rem(my_tp + step, tp_size)), device_id_type=MESH
        )
    for copy in small_copies:
        copy.wait()
    pl.semaphore_wait(barrier, ep_size + tp_size - 2)

    def ep_copy(number, step, owner):
        target = small[number][1]
        return pltpu.make_async_remote_copy(
            src_ref=token_slot(target, owner),
            dst_ref=token_slot(target, owner),
            send_sem=send_sem.at[number, step - 1],
            recv_sem=recv_sem.at[number, step - 1],
            device_id=(lax.rem(my_ep + step, ep_size), my_tp),
            device_id_type=MESH,
        )

    def source_ep(step):
        return lax.rem(my_ep + ep_size - step, ep_size)

    for number in range(3):
        for step in range(1, ep_size):
            ep_copy(number, step, my_ep).start()

    for step in range(1, ep_size):
        ep_copy(0, step, source_ep(step)).wait_recv()
    key_copy.wait()

    token_vectors = features[...]

    def dense_step(index, carry):
        for inner in range(GROUP):
            block = index * GROUP + inner
            rows = key[pl.ds(pl.multiple_of(block * LANES, LANES), LANES), :]
            dense[pl.ds(pl.multiple_of(block * tokens, tokens), tokens), :] = matmul_nt(
                token_vectors, rows
            )
        return carry

    lax.fori_loop(0, blocks // GROUP, dense_step, 0)

    for step in range(1, ep_size):
        ep_copy(1, step, source_ep(step)).wait_recv()

    def packed(pieces):
        flat = jnp.concatenate(pieces, axis=1)
        return jnp.concatenate([flat[:half], flat[half:]], axis=1)

    picks[...] = packed([chosen[:, head, :] for head in range(heads)]) - my_ep * table_rows

    block_ids = lax.broadcasted_iota(jnp.int32, (blocks, width), 0)
    lane_ids = lax.broadcasted_iota(jnp.int32, (LANES, width), 0)
    in_first = lax.broadcasted_iota(jnp.int32, (blocks, width), 1) < per_token

    def masks(pair):
        row = picks[pl.ds(pair, 1), :]
        column_hot = jnp.where((row & (LANES - 1)) == lane_ids, 1.0, 0.0).astype(jnp.bfloat16)
        block_mask = lax.shift_right_arithmetic(row, 7) == block_ids
        return column_hot, block_mask

    def chosen_of(token, column_hot):
        upper, lower = split_terms(dense[pl.ds(token, blocks, stride=tokens), :])
        return jnp.dot(upper, column_hot, preferred_element_type=jnp.float32) + jnp.dot(
            lower, column_hot, preferred_element_type=jnp.float32
        )

    def pick_step(pair, carry):
        column_hot, block_mask = masks(pair)
        both = jnp.where(
            in_first, chosen_of(pair, column_hot), chosen_of(pair + half, column_hot)
        )
        partial[my_tp, pl.ds(pair, 1), :] = jnp.sum(
            jnp.where(block_mask, both, 0.0), axis=0, keepdims=True
        )
        return carry

    lax.fori_loop(0, half, pick_step, 0, unroll=2)

    def tp_copy(step, owner):
        return pltpu.make_async_remote_copy(
            src_ref=partial.at[owner],
            dst_ref=partial.at[owner],
            send_sem=tp_send.at[step - 1],
            recv_sem=tp_recv.at[step - 1],
            device_id=(my_ep, lax.rem(my_tp + step, tp_size)),
            device_id_type=MESH,
        )

    for step in range(1, tp_size):
        tp_copy(step, my_tp).start()

    for step in range(1, ep_size):
        ep_copy(2, step, source_ep(step)).wait_recv()
    gate_pieces = []
    for head in range(heads):
        logits = scores[:, head, :]
        powers = jnp.exp(logits - jnp.max(logits, axis=1, keepdims=True))
        gate_pieces.append(powers / jnp.sum(powers, axis=1, keepdims=True))
    gates = packed(gate_pieces)

    for step in range(1, tp_size):
        tp_copy(step, lax.rem(my_tp + tp_size - step, tp_size)).wait_recv()
    products = partial[0]
    for index in range(1, tp_size):
        products = products + partial[index]
    activated = 0.5 * products * (1.0 + lax.erf(products * (0.5**0.5)))
    weights[...] = (gates * activated).astype(jnp.bfloat16).astype(jnp.float32)

    def spread_step(pair, carry):
        column_hot, block_mask = masks(pair)
        hot = jnp.where(block_mask, weights[pl.ds(pair, 1), :], 0.0)
        for token, keep in ((pair, in_first), (pair + half, jnp.logical_not(in_first))):
            dense[pl.ds(token, blocks, stride=tokens), :] = matmul_nt(
                jnp.where(keep, hot, 0.0).astype(jnp.bfloat16), column_hot
            )
        return carry

    lax.fori_loop(0, half, spread_step, 0, unroll=2)

    value_copy.wait()

    def value_step(index, total):
        for inner in range(GROUP):
            block = index * GROUP + inner
            rows = value[pl.ds(pl.multiple_of(block * LANES, LANES), LANES), :]
            upper, lower = split_terms(
                dense[pl.ds(pl.multiple_of(block * tokens, tokens), tokens), :]
            )
            total = total + jnp.dot(upper, rows, preferred_element_type=jnp.float32)
            total = total + jnp.dot(lower, rows, preferred_element_type=jnp.float32)
        return total

    zero = jnp.zeros(summed.shape, jnp.float32)
    summed[...] = lax.fori_loop(0, blocks // GROUP, value_step, zero)

    def out_copy(step, owner):
        return pltpu.make_async_remote_copy(
            src_ref=token_slot(summed, lax.rem(my_ep + step, ep_size)),
            dst_ref=landed.at[step - 1],
            send_sem=out_send.at[step - 1],
            recv_sem=out_recv.at[step - 1],
            device_id=(lax.rem(my_ep + step, ep_size), my_tp),
            device_id_type=MESH,
        )

    for step in range(1, ep_size):
        out_copy(step, my_ep).start()
    result = summed[pl.ds(pl.multiple_of(my_ep * own_tokens, own_tokens), own_tokens), :]
    for step in range(1, ep_size):
        out_copy(step, my_ep).wait_recv()
        result = result + landed[step - 1]
    out_ref[...] = result.astype(out_ref.dtype)

    for step in range(1, ep_size):
        for number in range(3):
            ep_copy(number, step, my_ep).wait_send()
        out_copy(step, my_ep).wait_send()
    for step in range(1, tp_size):
        tp_copy(step, my_tp).wait_send()


def shards(ep_size, tp_size, features, key_table, value_table, chosen, scores):
    own_tokens, width = features.shape
    _, heads, top = chosen.shape
    table_rows = key_table.shape[0]
    tokens = ep_size * own_tokens
    packed_shape = (tokens // 2, 2 * heads * top)
    dma = pltpu.SemaphoreType.DMA
    return pl.pallas_call(
        functools.partial(kernel, ep_size, tp_size),
        out_shape=jax.ShapeDtypeStruct((own_tokens, width), jnp.bfloat16),
        in_specs=[pl.BlockSpec(memory_space=pl.ANY)] * 5,
        out_specs=pl.BlockSpec(memory_space=pltpu.VMEM),
        scratch_shapes=[
            pltpu.VMEM((tokens, width), features.dtype),
            pltpu.VMEM((tokens, heads, top), jnp.int32),
            pltpu.VMEM((tokens, heads, top), jnp.float32),
            pltpu.VMEM((table_rows, width), key_table.dtype),
            pltpu.VMEM((table_rows, width), value_table.dtype),
            pltpu.VMEM((table_rows // LANES * tokens, LANES), jnp.float32),
            pltpu.VMEM(packed_shape, jnp.int32),
            pltpu.VMEM((tp_size,) + packed_shape, jnp.float32),
            pltpu.VMEM(packed_shape, jnp.float32),
            pltpu.VMEM((tokens, width), jnp.float32),
            pltpu.VMEM((ep_size - 1, own_tokens, width), jnp.float32),
            dma((5,)),
            dma((3, ep_size - 1)),
            dma((3, ep_size - 1)),
            dma((tp_size - 1,)),
            dma((tp_size - 1,)),
            dma((ep_size - 1,)),
            dma((ep_size - 1,)),
        ],
        compiler_params=pltpu.CompilerParams(collective_id=0, has_side_effects=True),
    )(features, key_table, value_table, chosen, scores)


def solution(mesh):
    return jax.shard_map(
        functools.partial(shards, mesh.shape["ep"], mesh.shape["tp"]),
        mesh=mesh,
        in_specs=(
            P("ep", "tp"),
            P("ep", "tp"),
            P("ep", "tp"),
            P("ep", None, None),
            P("ep", None, None),
        ),
        out_specs=P("ep", "tp"),
        check_vma=False,
    )
```

time: 151 us -> 38.8 us (0.26)
  blocking collectives: 66.6 us -> 0 us
  local copies, waits for them, and re-layouts: 40 us -> 1.28 us
  Pallas kernels: 0 us -> 37.3 us
  other arithmetic: 27.5 us -> 0 us
  matrix products: 15.2 us -> 0 us
    pallas_call x0 -> x1, Pallas kernels: none -> 37.3 us  [shards(): pl.pallas_call(functools.partial(kernel, ep_size, tp_size), out_shape=jax...]
    gather x6 -> x0, local copies, waits for them, and re-layouts: 33.6 us -> none  [dots_block(): return jnp.take_along_axis(dense, picked, axis=1)]
    while x8 -> x0, other arithmetic: 27.1 us -> none
    psum x1 -> x0, blocking collectives: 26 us -> none  [shards(): products = lax.psum(partial_value, 'tp')]
    all_gather x3 -> x0, blocking collectives: 25.8 us -> none  [the longest x1 10.2 us: shards(): chosen_all = lax.all_gather(chosen, 'ep', axis=0, tiled=True)]
    dot_general x6 -> x0, matrix products: 15.2 us -> none  [the longest x2 7.46 us: dots_block(): lax.dot_general(token_block, key_table, (((1,), (1,)), ((), ())), preferr...]
    unnamed x1 -> x0, blocking collectives: 14.8 us -> none
    scatter-add x2 -> x0, local copies, waits for them, and re-layouts: 3.49 us -> none  [value_block(): dense = jnp.zeros((width, table_rows), jnp.float32).at[token_ids, picked]...]
where the time goes in v1:
time: 38.8 us; the launch traced here: 38.6 us
  Pallas kernels  37.3 us (96%)
  local copies, waits for them, and re-layouts  1.28 us (3%)
    pallas_call x1, Pallas kernels, shards(): pl.pallas_call(functools.partial(kernel, ep_size, tp_size), out_shape=jax...  37.3 us
    unnamed x1, local copies, waits for them, and re-layouts  1.28 us

profile of v1, /device:TPU:0, one launch (start us, length us, event | category | flops | bytes accessed | tf_op | source)
XLA Modules:
  0.0 38.6 jit_solution(11535803148630745608)
XLA Ops:
  0.0 37.3 %shard_map.55 = bf16[16,128]{1,0:T(8,128)(2,1)} custom-call(bf16[16,128]{1,0:T(8,128)(2,1)} %features_hbm.1, bf16[16384,128]{1,0:T(8,128)(2,1)} %key_hbm.1, bf16[16384,128]{1,0:T(8,128)(2,1)} %value_hbm.1, s32[16,4,16]{2,1,0:T(4,128)} %chosen_hbm.1, f32[16,4,16]{2,1,0:T(4,128)} %scores_hbm.1), custom_call_target="tpu_custom_call" | custom-call | tf_op jit(solution)/shard_map/pallas_call | solution.py:258
  37.3 1.3 %copy.7 = bf16[16,128]{1,0:T(8,128)(2,1)} copy(bf16[16,128]{1,0:T(8,128)(2,1)} %shard_map.55) | data formatting | bytes 8192

commit v2 on v1

--- a/solution.py
+++ b/solution.py
@@ -9,6 +9,7 @@
 
 LANES = 128
 GROUP = 16
+PITCH_PAD = 4
 MESH = pl.DeviceIdType.MESH
 
 
@@ -59,6 +60,7 @@
     own_tokens, heads, top = chosen_hbm.shape
     tokens = ep_size * own_tokens
     half = tokens // 2
+    pitch = tokens + PITCH_PAD
     per_token = heads * top
     width = 2 * per_token
 
@@ -121,7 +123,7 @@
         for inner in range(GROUP):
             block = index * GROUP + inner
             rows = key[pl.ds(pl.multiple_of(block * LANES, LANES), LANES), :]
-            dense[pl.ds(pl.multiple_of(block * tokens, tokens), tokens), :] = matmul_nt(
+            dense[pl.ds(block * pitch, tokens), :] = matmul_nt(
                 token_vectors, rows
             )
         return carry
@@ -148,7 +150,7 @@
         return column_hot, block_mask
 
     def chosen_of(token, column_hot):
-        upper, lower = split_terms(dense[pl.ds(token, blocks, stride=tokens), :])
+        upper, lower = split_terms(dense[pl.ds(token, blocks, stride=pitch), :])
         return jnp.dot(upper, column_hot, preferred_element_type=jnp.float32) + jnp.dot(
             lower, column_hot, preferred_element_type=jnp.float32
         )
@@ -199,7 +201,7 @@
         column_hot, block_mask = masks(pair)
         hot = jnp.where(block_mask, weights[pl.ds(pair, 1), :], 0.0)
         for token, keep in ((pair, in_first), (pair + half, jnp.logical_not(in_first))):
-            dense[pl.ds(token, blocks, stride=tokens), :] = matmul_nt(
+            dense[pl.ds(token, blocks, stride=pitch), :] = matmul_nt(
                 jnp.where(keep, hot, 0.0).astype(jnp.bfloat16), column_hot
             )
         return carry
@@ -213,14 +215,15 @@
             block = index * GROUP + inner
             rows = value[pl.ds(pl.multiple_of(block * LANES, LANES), LANES), :]
             upper, lower = split_terms(
-                dense[pl.ds(pl.multiple_of(block * tokens, tokens), tokens), :]
+                dense[pl.ds(block * pitch, tokens), :]
             )
-            total = total + jnp.dot(upper, rows, preferred_element_type=jnp.float32)
-            total = total + jnp.dot(lower, rows, preferred_element_type=jnp.float32)
+            both = jnp.concatenate([upper, lower], axis=0)
+            total = total + jnp.dot(both, rows, preferred_element_type=jnp.float32)
         return total
 
-    zero = jnp.zeros(summed.shape, jnp.float32)
-    summed[...] = lax.fori_loop(0, blocks // GROUP, value_step, zero)
+    zero = jnp.zeros((2 * tokens, summed.shape[1]), jnp.float32)
+    total = lax.fori_loop(0, blocks // GROUP, value_step, zero)
+    summed[...] = total[:tokens] + total[tokens:]
 
     def out_copy(step, owner):
         return pltpu.make_async_remote_copy(
@@ -266,7 +269,7 @@
             pltpu.VMEM((tokens, heads, top), jnp.float32),
             pltpu.VMEM((table_rows, width), key_table.dtype),
             pltpu.VMEM((table_rows, width), value_table.dtype),
-            pltpu.VMEM((table_rows // LANES * tokens, LANES), jnp.float32),
+            pltpu.VMEM((table_rows // LANES * (tokens + PITCH_PAD), LANES), jnp.float32),
             pltpu.VMEM(packed_shape, jnp.int32),
             pltpu.VMEM((tp_size,) + packed_shape, jnp.float32),
             pltpu.VMEM(packed_shape, jnp.float32),

time: 38.8 us -> 31.4 us (0.81)
  Pallas kernels: 37.3 us -> 29.9 us
    pallas_call x1, Pallas kernels: 37.3 us -> 29.9 us  [shards(): pl.pallas_call(functools.partial(kernel, ep_size, tp_size), out_shape=jax...]
where the time goes in v2:
time: 31.4 us; the launch traced here: 31.2 us
  Pallas kernels  29.9 us (95%)
  local copies, waits for them, and re-layouts  1.28 us (4%)
    pallas_call x1, Pallas kernels, shards(): pl.pallas_call(functools.partial(kernel, ep_size, tp_size), out_shape=jax...  29.9 us
    unnamed x1, local copies, waits for them, and re-layouts  1.28 us

profile of v2, /device:TPU:0, one launch (start us, length us, event | category | flops | bytes accessed | tf_op | source)
XLA Modules:
  0.0 31.2 jit_solution(6961257481951052436)
XLA Ops:
  0.0 29.9 %shard_map.55 = bf16[16,128]{1,0:T(8,128)(2,1)} custom-call(bf16[16,128]{1,0:T(8,128)(2,1)} %features_hbm.1, bf16[16384,128]{1,0:T(8,128)(2,1)} %key_hbm.1, bf16[16384,128]{1,0:T(8,128)(2,1)} %value_hbm.1, s32[16,4,16]{2,1,0:T(4,128)} %chosen_hbm.1, f32[16,4,16]{2,1,0:T(4,128)} %scores_hbm.1), custom_call_target="tpu_custom_call" | custom-call | tf_op jit(solution)/shard_map/pallas_call | solution.py:261
  29.9 1.3 %copy.7 = bf16[16,128]{1,0:T(8,128)(2,1)} copy(bf16[16,128]{1,0:T(8,128)(2,1)} %shard_map.55) | data formatting | bytes 8192

commit v3 on v2

--- a/solution.py
+++ b/solution.py
@@ -8,7 +8,7 @@
 from jax.sharding import PartitionSpec as P
 
 LANES = 128
-GROUP = 16
+GROUP = 64
 PITCH_PAD = 4
 MESH = pl.DeviceIdType.MESH
 
@@ -37,10 +37,11 @@
     features,
     chosen,
     scores,
+    picks,
+    gates,
     key,
     value,
     dense,
-    picks,
     partial,
     weights,
     summed,
@@ -59,7 +60,7 @@
     blocks = table_rows // LANES
     own_tokens, heads, top = chosen_hbm.shape
     tokens = ep_size * own_tokens
-    half = tokens // 2
+    own_pairs = own_tokens // 2
     pitch = tokens + PITCH_PAD
     per_token = heads * top
     width = 2 * per_token
@@ -67,14 +68,17 @@
     def token_slot(ref, index):
         return ref.at[pl.ds(index * own_tokens, own_tokens)]
 
+    def pair_slot(ref, index):
+        return ref.at[pl.ds(pl.multiple_of(index * own_pairs, own_pairs), own_pairs)]
+
     small = (
-        (features_hbm, features),
+        (features_hbm, token_slot(features, my_ep)),
         (chosen_hbm, chosen),
         (scores_hbm, scores),
     )
     small_copies = []
     for number, (source, target) in enumerate(small):
-        copy = pltpu.make_async_copy(source, token_slot(target, my_ep), local_sem.at[number])
+        copy = pltpu.make_async_copy(source, target, local_sem.at[number])
         copy.start()
         small_copies.append(copy)
     key_copy = pltpu.make_async_copy(key_hbm, key, local_sem.at[3])
@@ -93,13 +97,29 @@
         )
     for copy in small_copies:
         copy.wait()
+
+    def packed(pieces):
+        flat = jnp.concatenate(pieces, axis=1)
+        return jnp.concatenate([flat[:own_pairs], flat[own_pairs:]], axis=1)
+
+    pair_slot(picks, my_ep)[...] = packed([chosen[:, head, :] for head in range(heads)])
+    gate_pieces = []
+    for head in range(heads):
+        logits = scores[:, head, :]
+        powers = jnp.exp(logits - jnp.max(logits, axis=1, keepdims=True))
+        gate_pieces.append(powers / jnp.sum(powers, axis=1, keepdims=True))
+    pair_slot(gates, my_ep)[...] = packed(gate_pieces)
     pl.semaphore_wait(barrier, ep_size + tp_size - 2)
 
     def ep_copy(number, step, owner):
-        target = small[number][1]
+        slot = (
+            token_slot(features, owner),
+            pair_slot(picks, owner),
+            pair_slot(gates, owner),
+        )[number]
         return pltpu.make_async_remote_copy(
-            src_ref=token_slot(target, owner),
-            dst_ref=token_slot(target, owner),
+            src_ref=slot,
+            dst_ref=slot,
             send_sem=send_sem.at[number, step - 1],
             recv_sem=recv_sem.at[number, step - 1],
             device_id=(lax.rem(my_ep + step, ep_size), my_tp),
@@ -133,18 +153,13 @@
     for step in range(1, ep_size):
         ep_copy(1, step, source_ep(step)).wait_recv()
 
-    def packed(pieces):
-        flat = jnp.concatenate(pieces, axis=1)
-        return jnp.concatenate([flat[:half], flat[half:]], axis=1)
-
-    picks[...] = packed([chosen[:, head, :] for head in range(heads)]) - my_ep * table_rows
-
+    first_row = my_ep * table_rows
     block_ids = lax.broadcasted_iota(jnp.int32, (blocks, width), 0)
     lane_ids = lax.broadcasted_iota(jnp.int32, (LANES, width), 0)
     in_first = lax.broadcasted_iota(jnp.int32, (blocks, width), 1) < per_token
 
     def masks(pair):
-        row = picks[pl.ds(pair, 1), :]
+        row = picks[pl.ds(pair, 1), :] - first_row
         column_hot = jnp.where((row & (LANES - 1)) == lane_ids, 1.0, 0.0).astype(jnp.bfloat16)
         block_mask = lax.shift_right_arithmetic(row, 7) == block_ids
         return column_hot, block_mask
@@ -155,17 +170,22 @@
             lower, column_hot, preferred_element_type=jnp.float32
         )
 
-    def pick_step(pair, carry):
-        column_hot, block_mask = masks(pair)
-        both = jnp.where(
-            in_first, chosen_of(pair, column_hot), chosen_of(pair + half, column_hot)
-        )
-        partial[my_tp, pl.ds(pair, 1), :] = jnp.sum(
-            jnp.where(block_mask, both, 0.0), axis=0, keepdims=True
-        )
+    def pick_step(owner, carry):
+        for inner in range(own_pairs):
+            pair = owner * own_pairs + inner
+            token = owner * own_tokens + inner
+            column_hot, block_mask = masks(pair)
+            both = jnp.where(
+                in_first,
+                chosen_of(token, column_hot),
+                chosen_of(token + own_pairs, column_hot),
+            )
+            partial[my_tp, pl.ds(pair, 1), :] = jnp.sum(
+                jnp.where(block_mask, both, 0.0), axis=0, keepdims=True
+            )
         return carry
 
-    lax.fori_loop(0, half, pick_step, 0, unroll=2)
+    lax.fori_loop(0, ep_size, pick_step, 0)
 
     def tp_copy(step, owner):
         return pltpu.make_async_remote_copy(
@@ -182,31 +202,30 @@
 
     for step in range(1, ep_size):
         ep_copy(2, step, source_ep(step)).wait_recv()
-    gate_pieces = []
-    for head in range(heads):
-        logits = scores[:, head, :]
-        powers = jnp.exp(logits - jnp.max(logits, axis=1, keepdims=True))
-        gate_pieces.append(powers / jnp.sum(powers, axis=1, keepdims=True))
-    gates = packed(gate_pieces)
-
     for step in range(1, tp_size):
         tp_copy(step, lax.rem(my_tp + tp_size - step, tp_size)).wait_recv()
     products = partial[0]
     for index in range(1, tp_size):
         products = products + partial[index]
     activated = 0.5 * products * (1.0 + lax.erf(products * (0.5**0.5)))
-    weights[...] = (gates * activated).astype(jnp.bfloat16).astype(jnp.float32)
-
-    def spread_step(pair, carry):
-        column_hot, block_mask = masks(pair)
-        hot = jnp.where(block_mask, weights[pl.ds(pair, 1), :], 0.0)
-        for token, keep in ((pair, in_first), (pair + half, jnp.logical_not(in_first))):
-            dense[pl.ds(token, blocks, stride=pitch), :] = matmul_nt(
-                jnp.where(keep, hot, 0.0).astype(jnp.bfloat16), column_hot
-            )
+    weights[...] = (gates[...] * activated).astype(jnp.bfloat16).astype(jnp.float32)
+
+    def spread_step(owner, carry):
+        for inner in range(own_pairs):
+            pair = owner * own_pairs + inner
+            first = owner * own_tokens + inner
+            column_hot, block_mask = masks(pair)
+            hot = jnp.where(block_mask, weights[pl.ds(pair, 1), :], 0.0)
+            for token, keep in (
+                (first, in_first),
+                (first + own_pairs, jnp.logical_not(in_first)),
+            ):
+                dense[pl.ds(token, blocks, stride=pitch), :] = matmul_nt(
+                    jnp.where(keep, hot, 0.0).astype(jnp.bfloat16), column_hot
+                )
         return carry
 
-    lax.fori_loop(0, half, spread_step, 0, unroll=2)
+    lax.fori_loop(0, ep_size, spread_step, 0)
 
     value_copy.wait()
 
@@ -260,17 +279,18 @@
     dma = pltpu.SemaphoreType.DMA
     return pl.pallas_call(
         functools.partial(kernel, ep_size, tp_size),
-        out_shape=jax.ShapeDtypeStruct((own_tokens, width), jnp.bfloat16),
+        out_shape=pltpu.VMEM((own_tokens, width), jnp.bfloat16),
         in_specs=[pl.BlockSpec(memory_space=pl.ANY)] * 5,
         out_specs=pl.BlockSpec(memory_space=pltpu.VMEM),
         scratch_shapes=[
             pltpu.VMEM((tokens, width), features.dtype),
-            pltpu.VMEM((tokens, heads, top), jnp.int32),
-            pltpu.VMEM((tokens, heads, top), jnp.float32),
+            pltpu.VMEM((own_tokens, heads, top), jnp.int32),
+            pltpu.VMEM((own_tokens, heads, top), jnp.float32),
+            pltpu.VMEM(packed_shape, jnp.int32),
+            pltpu.VMEM(packed_shape, jnp.float32),
             pltpu.VMEM((table_rows, width), key_table.dtype),
             pltpu.VMEM((table_rows, width), value_table.dtype),
             pltpu.VMEM((table_rows // LANES * (tokens + PITCH_PAD), LANES), jnp.float32),
-            pltpu.VMEM(packed_shape, jnp.int32),
             pltpu.VMEM((tp_size,) + packed_shape, jnp.float32),
             pltpu.VMEM(packed_shape, jnp.float32),
             pltpu.VMEM((tokens, width), jnp.float32),

time: 31.4 us -> 25 us (0.80)
  Pallas kernels: 29.9 us -> 24.2 us
  local copies, waits for them, and re-layouts: 1.28 us -> 0.6 us
    pallas_call x1, Pallas kernels: 29.9 us -> 24.2 us  [shards(): pl.pallas_call(functools.partial(kernel, ep_size, tp_size), out_shape=plt...]
    unnamed x1, local copies, waits for them, and re-layouts: 1.28 us -> 0.6 us
where the time goes in v3:
time: 25 us; the launch traced here: 24.8 us
  Pallas kernels  24.2 us (97%)
  local copies, waits for them, and re-layouts  0.6 us (2%)
    pallas_call x1, Pallas kernels, shards(): pl.pallas_call(functools.partial(kernel, ep_size, tp_size), out_shape=plt...  24.2 us
    unnamed x1, local copies, waits for them, and re-layouts  0.6 us

profile of v3, /device:TPU:0, one launch (start us, length us, event | category | flops | bytes accessed | tf_op | source)
XLA Modules:
  0.0 24.8 jit_solution(7369277867781496208)
XLA Ops:
  0.0 24.2 %shard_map.55 = bf16[16,128]{1,0:T(8,128)(2,1)S(1)} custom-call(bf16[16,128]{1,0:T(8,128)(2,1)} %features_hbm.1, bf16[16384,128]{1,0:T(8,128)(2,1)} %key_hbm.1, bf16[16384,128]{1,0:T(8,128)(2,1)} %value_hbm.1, s32[16,4,16]{2,1,0:T(4,128)} %chosen_hbm.1, f32[16,4,16]{2,1,0:T(4,128)} %scores_hbm.1), custom_call_target="tpu_custom_call" | custom-call | tf_op jit(solution)/shard_map/pallas_call | solution.py:280
  24.2 0.6 %copy.7 = bf16[16,128]{1,0:T(8,128)(2,1)} copy(bf16[16,128]{1,0:T(8,128)(2,1)S(1)} %shard_map.55) | data formatting | bytes 8192

commit v4 on v3

--- a/solution.py
+++ b/solution.py
@@ -10,6 +10,7 @@
 LANES = 128
 GROUP = 64
 PITCH_PAD = 4
+CHUNKS = 4
 MESH = pl.DeviceIdType.MESH
 
 
@@ -23,6 +24,10 @@
     upper = value.astype(jnp.bfloat16)
     lower = (value - upper.astype(jnp.float32)).astype(jnp.bfloat16)
     return upper, lower
+
+
+def chunk_count(ep_size):
+    return CHUNKS if ep_size % CHUNKS == 0 else 1
 
 
 def kernel(
@@ -40,6 +45,7 @@
     picks,
     gates,
     key,
+    key_columns,
     value,
     dense,
     partial,
@@ -61,6 +67,9 @@
     own_tokens, heads, top = chosen_hbm.shape
     tokens = ep_size * own_tokens
     own_pairs = own_tokens // 2
+    chunks = chunk_count(ep_size)
+    chunk_owners = ep_size // chunks
+    chunk_pairs = chunk_owners * own_pairs
     pitch = tokens + PITCH_PAD
     per_token = heads * top
     width = 2 * per_token
@@ -133,18 +142,28 @@
         for step in range(1, ep_size):
             ep_copy(number, step, my_ep).start()
 
+    depth = key.shape[1]
+
+    def turn_step(index, carry):
+        for inner in range(GROUP):
+            block = index * GROUP + inner
+            rows = key[pl.ds(pl.multiple_of(block * LANES, LANES), LANES), :]
+            key_columns[pl.ds(pl.multiple_of(block * depth, depth), depth), :] = rows.T
+        return carry
+
+    key_copy.wait()
+    lax.fori_loop(0, blocks // GROUP, turn_step, 0)
+
     for step in range(1, ep_size):
         ep_copy(0, step, source_ep(step)).wait_recv()
-    key_copy.wait()
-
     token_vectors = features[...]
 
     def dense_step(index, carry):
         for inner in range(GROUP):
             block = index * GROUP + inner
-            rows = key[pl.ds(pl.multiple_of(block * LANES, LANES), LANES), :]
-            dense[pl.ds(block * pitch, tokens), :] = matmul_nt(
-                token_vectors, rows
+            columns = key_columns[pl.ds(pl.multiple_of(block * depth, depth), depth), :]
+            dense[pl.ds(block * pitch, tokens), :] = jnp.dot(
+                token_vectors, columns, preferred_element_type=jnp.float32
             )
         return carry
 
@@ -168,6 +187,20 @@
         upper, lower = split_terms(dense[pl.ds(token, blocks, stride=pitch), :])
         return jnp.dot(upper, column_hot, preferred_element_type=jnp.float32) + jnp.dot(
             lower, column_hot, preferred_element_type=jnp.float32
+        )
+
+    def chunk_rows(chunk):
+        return pl.ds(pl.multiple_of(chunk * chunk_pairs, chunk_pairs), chunk_pairs)
+
+    def tp_copy(step, owner, chunk):
+        slot = partial.at[owner, chunk_rows(chunk)]
+        return pltpu.make_async_remote_copy(
+            src_ref=slot,
+            dst_ref=slot,
+            send_sem=tp_send.at[step - 1, chunk],
+            recv_sem=tp_recv.at[step - 1, chunk],
+            device_id=(my_ep, lax.rem(my_tp + step, tp_size)),
+            device_id_type=MESH,
         )
 
     def pick_step(owner, carry):
@@ -185,31 +218,20 @@
             )
         return carry
 
-    lax.fori_loop(0, ep_size, pick_step, 0)
-
-    def tp_copy(step, owner):
-        return pltpu.make_async_remote_copy(
-            src_ref=partial.at[owner],
-            dst_ref=partial.at[owner],
-            send_sem=tp_send.at[step - 1],
-            recv_sem=tp_recv.at[step - 1],
-            device_id=(my_ep, lax.rem(my_tp + step, tp_size)),
-            device_id_type=MESH,
-        )
-
-    for step in range(1, tp_size):
-        tp_copy(step, my_tp).start()
+    def pick_chunk(chunk, carry):
+        if chunk_owners == 1:
+            pick_step(chunk, 0)
+        else:
+            first = chunk * chunk_owners
+            lax.fori_loop(first, first + chunk_owners, pick_step, 0)
+        for step in range(1, tp_size):
+            tp_copy(step, my_tp, chunk).start()
+        return carry
+
+    lax.fori_loop(0, chunks, pick_chunk, 0)
 
     for step in range(1, ep_size):
         ep_copy(2, step, source_ep(step)).wait_recv()
-    for step in range(1, tp_size):
-        tp_copy(step, lax.rem(my_tp + tp_size - step, tp_size)).wait_recv()
-    products = partial[0]
-    for index in range(1, tp_size):
-        products = products + partial[index]
-    activated = 0.5 * products * (1.0 + lax.erf(products * (0.5**0.5)))
-    weights[...] = (gates[...] * activated).astype(jnp.bfloat16).astype(jnp.float32)
-
     def spread_step(owner, carry):
         for inner in range(own_pairs):
             pair = owner * own_pairs + inner
@@ -225,7 +247,24 @@
                 )
         return carry
 
-    lax.fori_loop(0, ep_size, spread_step, 0)
+    def spread_chunk(chunk, carry):
+        for step in range(1, tp_size):
+            tp_copy(step, lax.rem(my_tp + tp_size - step, tp_size), chunk).wait_recv()
+        rows = chunk_rows(chunk)
+        products = partial[0, rows, :]
+        for index in range(1, tp_size):
+            products = products + partial[index, rows, :]
+        activated = 0.5 * products * (1.0 + lax.erf(products * (0.5**0.5)))
+        row_weights = (gates[rows, :] * activated).astype(jnp.bfloat16)
+        weights[rows, :] = row_weights.astype(jnp.float32)
+        if chunk_owners == 1:
+            spread_step(chunk, 0)
+        else:
+            first = chunk * chunk_owners
+            lax.fori_loop(first, first + chunk_owners, spread_step, 0)
+        return carry
+
+    lax.fori_loop(0, chunks, spread_chunk, 0)
 
     value_copy.wait()
 
@@ -267,7 +306,8 @@
             ep_copy(number, step, my_ep).wait_send()
         out_copy(step, my_ep).wait_send()
     for step in range(1, tp_size):
-        tp_copy(step, my_tp).wait_send()
+        for chunk in range(chunks):
+            tp_copy(step, my_tp, chunk).wait_send()
 
 
 def shards(ep_size, tp_size, features, key_table, value_table, chosen, scores):
@@ -289,6 +329,7 @@
             pltpu.VMEM(packed_shape, jnp.int32),
             pltpu.VMEM(packed_shape, jnp.float32),
             pltpu.VMEM((table_rows, width), key_table.dtype),
+            pltpu.VMEM((table_rows // LANES * width, LANES), key_table.dtype),
             pltpu.VMEM((table_rows, width), value_table.dtype),
             pltpu.VMEM((table_rows // LANES * (tokens + PITCH_PAD), LANES), jnp.float32),
             pltpu.VMEM((tp_size,) + packed_shape, jnp.float32),
@@ -298,8 +339,8 @@
             dma((5,)),
             dma((3, ep_size - 1)),
             dma((3, ep_size - 1)),
-            dma((tp_size - 1,)),
-            dma((tp_size - 1,)),
+            dma((tp_size - 1, chunk_count(ep_size))),
+            dma((tp_size - 1, chunk_count(ep_size))),
             dma((ep_size - 1,)),
             dma((ep_size - 1,)),
         ],

time: 25 us -> 22.2 us (0.89)
  Pallas kernels: 24.2 us -> 21.4 us
    pallas_call x1, Pallas kernels: 24.2 us -> 21.4 us  [shards(): pl.pallas_call(functools.partial(kernel, ep_size, tp_size), out_shape=plt...]
where the time goes in v4:
time: 22.2 us; the launch traced here: 22 us
  Pallas kernels  21.4 us (96%)
  local copies, waits for them, and re-layouts  0.6 us (3%)
    pallas_call x1, Pallas kernels, shards(): pl.pallas_call(functools.partial(kernel, ep_size, tp_size), out_shape=plt...  21.4 us
    unnamed x1, local copies, waits for them, and re-layouts  0.6 us

profile of v4, /device:TPU:0, one launch (start us, length us, event | category | flops | bytes accessed | tf_op | source)
XLA Modules:
  0.0 22.0 jit_solution(11763529630202863494)
XLA Ops:
  0.0 21.4 %shard_map.55 = bf16[16,128]{1,0:T(8,128)(2,1)S(1)} custom-call(bf16[16,128]{1,0:T(8,128)(2,1)} %features_hbm.1, bf16[16384,128]{1,0:T(8,128)(2,1)} %key_hbm.1, bf16[16384,128]{1,0:T(8,128)(2,1)} %value_hbm.1, s32[16,4,16]{2,1,0:T(4,128)} %chosen_hbm.1, f32[16,4,16]{2,1,0:T(4,128)} %scores_hbm.1), custom_call_target="tpu_custom_call" | custom-call | tf_op jit(solution)/shard_map/pallas_call | solution.py:320
  21.4 0.6 %copy.7 = bf16[16,128]{1,0:T(8,128)(2,1)} copy(bf16[16,128]{1,0:T(8,128)(2,1)S(1)} %shard_map.55) | data formatting | bytes 8192
